TPU v7x, 32 devices: a whole 2x2x4 slice. The times are simulated.
32 devices in a mesh: grp: 2 (over y), ep: 4 (over z), tp: 4 (over x, core).
Axes of the slice: x: 2, y: 2, z: 4, core: 2. Of those that a mesh axis runs over, the one named last changes fastest.
Arguments:
- queries: bfloat16 [4096, 1024], P(('grp', 'ep'), 'tp'), parts along dimension 0, may hold values from -6 to 6
- key_rows: bfloat16 [4096, 512], P(('grp', 'ep'), 'tp'), parts along dimension 0, may hold values from -6 to 6
- value_rows: bfloat16 [4096, 512], P(('grp', 'ep'), 'tp'), parts along dimension 0, may hold values from -6 to 6
- query_gain: float32 [128], replicated, may hold values from 0.3 to 9
- key_gain: float32 [128], replicated, may hold values from 0.3 to 9
- log_forget: float32 [8, 4096], P('tp', 'grp'), parts along dimension 1, may hold values from -2048 to 0, as said below
- out_weight: bfloat16 [1024, 2048], P('tp'), may hold values from -0.1875 to 0.1875
- expert_rows: bfloat16 [4096, 2048], P(('grp', 'ep')), parts along dimension 0, may hold values from -6 to 6
- expert_gain: float32 [2048], replicated, may hold values from 0.1 to 1.9
- routes: int32 [2, 4096], P(None, ('grp', 'ep')), parts along dimension 1, may hold values from 0 to 31, as said below
- route_weight: float32 [2, 4096], P(None, ('grp', 'ep')), parts along dimension 1, may hold values from 0.1 to 1
- gate_weight: bfloat16 [32, 2048, 1024], P('ep', None, 'tp'), may hold values from -0.125 to 0.125
- up_weight: bfloat16 [32, 2048, 1024], P('ep', None, 'tp'), may hold values from -0.125 to 0.125
- down_weight: bfloat16 [32, 1024, 2048], P('ep', 'tp'), may hold values from -0.1875 to 0.1875
Outputs:
- mixer_out: bfloat16 [4096, 2048], P(('grp', 'ep', 'tp')), parts along dimension 0
- expert_out: bfloat16 [4096, 2048], P(('grp', 'ep'), 'tp'), parts along dimension 0
There are 2 independent parts, one for each index of `grp`. A program takes and returns all parts, laid end to end along the dimension named above; an argument that names none is the same for every part. Nothing has to cross between parts.
Inputs may be any that keep to these rules, and one draw needn't show every extreme that they name: `log_forget`: each head's values never rise along the positions. `routes`: the 2 experts of a token differ and lie in one group of 8 consecutive numbers. Among the tokens of one index of ep (512 consecutive tokens), no expert is named more than 48 times, and in every draw some experts are named exactly 48 times in every such block.
All inputs are finite; a program needn't handle non-finite values.
Results may differ from a plain program's by a relative error of at most 0.012.
The roundings to bfloat16 on the way count: a program that leaves them out, or rounds other values in their place, can miss the bound.
Values may be sent and summed in bfloat16 or wider, within the bound.
A program may use at most 128 MiB of HBM per device.

v0:
```python
import jax
import jax.numpy as jnp
from jax import lax
from jax.sharding import PartitionSpec as P

HEAD_SIZE = 128
EXPERTS = 32
TOP = 2


def head_norm(inputs, scale_gain):
    widened = inputs.astype(jnp.float32)
    factor = lax.rsqrt(jnp.mean(widened * widened, axis=-1, keepdims=True) + 1e-06)
    return widened * factor * scale_gain


def slot_table(chosen, experts_all, capacity):
    n_rows = chosen.shape[0]
    per_row = chosen.shape[1]
    flat_ids = chosen.reshape(-1)
    one_hot = (flat_ids[:, None] == jnp.arange(experts_all, dtype=jnp.int32)[None, :]).astype(
        jnp.int32
    )
    within = jnp.sum((jnp.cumsum(one_hot, axis=0) - 1) * one_hot, axis=1)
    slot_index = flat_ids * capacity + within
    row_of = jnp.arange(n_rows * per_row, dtype=jnp.int32) // per_row
    slot_owner = jnp.full((experts_all * capacity,), n_rows, jnp.int32).at[slot_index].set(row_of)
    return (slot_index.reshape(n_rows, per_row), slot_owner)


def mixer_half(queries, key_rows, value_rows, query_gain, key_gain, log_forget, out_weight):
    span_rows = queries.shape[0]
    heads_dev = queries.shape[1] // HEAD_SIZE
    kv_dev = key_rows.shape[1] // HEAD_SIZE
    group_ratio = heads_dev // kv_dev
    scale_qk = HEAD_SIZE ** (-0.5)
    q_normed = head_norm(
        queries.reshape(span_rows, kv_dev, group_ratio, HEAD_SIZE), query_gain
    ).astype(jnp.bfloat16)
    k_normed = head_norm(key_rows.reshape(span_rows, kv_dev, HEAD_SIZE), key_gain).astype(
        jnp.bfloat16
    )
    key_value = jnp.concatenate(
        [k_normed.reshape(span_rows, kv_dev * HEAD_SIZE), value_rows], axis=1
    )
    first_row = lax.axis_index("ep") * span_rows
    last_row = first_row + span_rows - 1
    query_pos = first_row + jnp.arange(span_rows, dtype=jnp.int32)
    query_gates = lax.dynamic_slice_in_dim(log_forget, first_row, span_rows, 1)
    query_gates = query_gates.T.reshape(span_rows, kv_dev, group_ratio)

    def add_block(running, kv_block, key_start):
        run_max, run_sum, run_acc = running
        block_len = kv_block.shape[0]
        k_block = kv_block[:, : kv_dev * HEAD_SIZE].reshape(block_len, kv_dev, HEAD_SIZE)
        v_block = kv_block[:, kv_dev * HEAD_SIZE :].reshape(block_len, kv_dev, HEAD_SIZE)
        key_gates = lax.dynamic_slice_in_dim(log_forget, key_start, block_len, 1)
        key_gates = key_gates.reshape(kv_dev, group_ratio, block_len)
        scores = (
            jnp.einsum("qgrd,kgd->qgrk", q_normed, k_block, preferred_element_type=jnp.float32)
            * scale_qk
        )
        scores = scores + query_gates[..., None] - key_gates[None]
        key_pos = key_start + jnp.arange(block_len, dtype=jnp.int32)
        visible = key_pos[None, :] <= query_pos[:, None]
        scores = jnp.where(visible[:, None, None, :], scores, -jnp.inf)
        new_max = jnp.maximum(run_max, jnp.max(scores, axis=-1))
        shrink = jnp.exp(run_max - new_max)
        weights = jnp.exp(scores - new_max[..., None])
        run_sum = shrink * run_sum + jnp.sum(weights, axis=-1)
        gathered = jnp.einsum(
            "qgrk,kgd->qgrd",
            weights.astype(jnp.bfloat16),
            v_block,
            preferred_element_type=jnp.float32,
        )
        return (new_max, run_sum, shrink[..., None] * run_acc + gathered)

    start_state = (
        jnp.full((span_rows, kv_dev, group_ratio), -jnp.inf, jnp.float32),
        jnp.zeros((span_rows, kv_dev, group_ratio), jnp.float32),
        jnp.zeros((span_rows, kv_dev, group_ratio, HEAD_SIZE), jnp.float32),
    )
    kv_piece = lax.all_gather(key_value, "ep", axis=0, tiled=True)
    block_len = min(kv_piece.shape[0], span_rows)
    n_blocks = kv_piece.shape[0] // block_len

    def one_block(block_number, running_in):
        key_start = block_number * block_len
        kv_block = lax.dynamic_slice_in_dim(kv_piece, block_number * block_len, block_len, 0)

        def take_block(running_now):
            return add_block(running_now, kv_block, key_start)

        def skip_block(running_now):
            return running_now

        return lax.cond(key_start <= last_row, take_block, skip_block, running_in)

    run_max, run_sum, run_acc = lax.fori_loop(0, n_blocks, one_block, start_state)
    attended = (
        (run_acc / run_sum[..., None])
        .astype(jnp.bfloat16)
        .reshape(span_rows, heads_dev * HEAD_SIZE)
    )
    return lax.psum_scatter(
        jnp.dot(attended, out_weight, preferred_element_type=jnp.float32).astype(jnp.bfloat16),
        "tp",
        scatter_dimension=0,
        tiled=True,
    )


def experts_half(
    expert_rows, expert_gain, routes, route_weight, gate_weight, up_weight, down_weight
):
    n_tp = lax.axis_size("tp")
    n_ep = lax.axis_size("ep")
    span_rows = expert_rows.shape[0]
    model_width = expert_rows.shape[1]
    exp_dev = gate_weight.shape[0]
    capacity = n_tp * ((3 * (span_rows // n_tp) * TOP + 2 * EXPERTS - 1) // (2 * EXPERTS))
    normed = head_norm(expert_rows, expert_gain).astype(jnp.bfloat16)
    slot_index, slot_owner = slot_table(routes.T, EXPERTS, capacity)
    padded = jnp.concatenate([normed, jnp.zeros((1, model_width), jnp.bfloat16)], axis=0)
    part_len = capacity // n_tp
    owner_part = lax.dynamic_slice_in_dim(
        slot_owner.reshape(EXPERTS, capacity), lax.axis_index("tp") * part_len, part_len, 1
    )
    send_rows = padded[owner_part].reshape(n_ep, exp_dev, part_len, model_width)
    arrived = lax.all_to_all(send_rows, "ep", split_axis=0, concat_axis=0, tiled=True)
    slot_rows = lax.all_gather(arrived, "tp", axis=2, tiled=True)
    gate_part = jnp.einsum(
        "nxcd,xdf->nxcf", slot_rows, gate_weight, preferred_element_type=jnp.float32
    )
    up_part = jnp.einsum("nxcd,xdf->nxcf", slot_rows, up_weight, preferred_element_type=jnp.float32)
    hidden = (jax.nn.silu(gate_part) * up_part).astype(jnp.bfloat16)
    partial_out = jnp.einsum(
        "nxcf,xfd->nxcd", hidden, down_weight, preferred_element_type=jnp.float32
    )
    summed = lax.psum_scatter(
        partial_out.astype(jnp.bfloat16), "tp", scatter_dimension=3, tiled=True
    )
    returned = lax.all_to_all(summed, "ep", split_axis=0, concat_axis=0, tiled=True)
    result_table = returned.reshape(EXPERTS * capacity, returned.shape[3])
    picked = result_table[slot_index]
    combined = jnp.sum(picked.astype(jnp.float32) * route_weight.T[..., None], axis=1)
    return combined.astype(jnp.bfloat16)


def on_device(
    queries,
    key_rows,
    value_rows,
    query_gain,
    key_gain,
    log_forget,
    out_weight,
    expert_rows,
    expert_gain,
    routes,
    route_weight,
    gate_weight,
    up_weight,
    down_weight,
):
    mixer_out = mixer_half(
        queries, key_rows, value_rows, query_gain, key_gain, log_forget, out_weight
    )
    expert_out = experts_half(
        expert_rows, expert_gain, routes, route_weight, gate_weight, up_weight, down_weight
    )
    return (mixer_out, expert_out)


def solution(mesh):
    in_specs = (
        P(("grp", "ep"), "tp"),
        P(("grp", "ep"), "tp"),
        P(("grp", "ep"), "tp"),
        P(),
        P(),
        P("tp", "grp"),
        P("tp", None),
        P(("grp", "ep"), None),
        P(),
        P(None, ("grp", "ep")),
        P(None, ("grp", "ep")),
        P("ep", None, "tp"),
        P("ep", None, "tp"),
        P("ep", "tp", None),
    )
    out_specs = (P(("grp", "ep", "tp"), None), P(("grp", "ep"), "tp"))
    return jax.shard_map(
        on_device, mesh=mesh, in_specs=in_specs, out_specs=out_specs, check_vma=False
    )
```

profile of v0, /device:TPU:0, one launch (start us, length us, event | category | flops | bytes accessed | tf_op | source)
XLA Modules:
  0.0 288.6 jit_solution(16937159695791661863)
XLA Ops:
  7.2 1.0 copy.33
  8.2 0.2 eq.29
  8.4 0.8 eq.25
  9.2 0.6 add_select_fusion
  9.7 0.7 fusion.41
  10.4 15.7 %reduce-window.6 = s32[32,8,128]{2,1,0:T(8,128)S(1)} reduce-window(s32[32,8,128]{2,1,0:T(8,128)} %fusion.41, s32[]{:T(128)} %copy.74), window={size=1x1x128 pad=0_0x0_0x127_0}, to_apply=%region_10.11 | reduce-window | flops 4161536 | bytes 262148 | tf_op jit(solution)/shard_map/reduce-window
  26.1 0.8 slice.22
  26.9 1.0 copy.34
  27.9 0.6 slice.23
  28.5 0.8 copy.35
  29.4 0.7 fusion.40
  30.1 0.9 reduce_sum.65
  31.0 1.8 compare_select_fusion
  32.8 1.1 mul.179
  33.9 4.5 %scatter_custom_fusion = s32[1536]{0:T(1024)S(1)} fusion(s32[1024]{0:T(1024)S(1)} %bitcast.122, s32[1024]{0:T(1024)} %add_select_fusion, s32[]{:T(128)} %constant.115.clone.1), kind=kCustom, calls=%fused_computation.79 | custom fusion | bytes 6656 | tf_op jit(solution)/shard_map/scatter | solution.py:27
  38.7 0.5 fusion.22
  39.2 0.5 fusion.24
  39.8 0.2 concatenate.7
  40.0 3.1 %gather_fusion = bf16[384,2048]{1,0:T(8,128)(2,1)} fusion(bf16[513,2048]{1,0:T(8,128)(2,1)S(1)} %concatenate.7, s32[1024]{0:T(1024)S(1)} %pad_clamp_fusion), kind=kCustom, calls=%fused_computation | custom fusion | bytes 3147264 | tf_op jit(solution)/shard_map/gather | solution.py:130
  43.1 2.4 reshape.235
  45.5 0.9 copy.36
  46.4 43.1 %all_to_all.10 = bf16[4,8,12,2048]{3,1,2,0:T(8,128)(2,1)S(1)} all-to-all(bf16[4,8,12,2048]{3,1,2,0:T(8,128)(2,1)S(1)} %copy.36), channel_id=1, replica_groups=mesh['grp'=2,'ep'=4,'tp'=4] {'ep'}, dimensions={0} | all-to-all | bytes 3145728 | tf_op jit(solution)/shard_map/all_to_all | solution.py:131
  89.5 1.2 copy.37
  91.2 0.7 pad_maximum_fusion
  91.9 0.2 reduce-scatter.5.cloned.1.call-start
  92.1 44.3 %all-gather.5.cloned.1.call-done = bf16[4,8,48,2048]{3,1,0,2:T(8,128)(2,1)} async-done(((bf16[4,8,12,2048]{3,1,0,2:T(8,128)(2,1)}), bf16[4,8,48,2048]{3,1,0,2:T(8,128)(2,1)}) %all-gather.5.cloned.1.call-update) | async-done | bytes 6291472 | tf_op jit(solution)/shard_map/all_gather | solution.py:132
  136.4 9.3 %fusion.16 = f32[8,4,48,256]{3,2,1,0:T(8,128)S(1)} fusion(bf16[8,2048,256]{2,1,0:T(8,128)(2,1)} %param.29, bf16[4,8,48,2048]{3,1,0,2:T(8,128)(2,1)} %all-gather.5.cloned.1.call-done), kind=kOutput, calls=%fused_computation.30 | convolution fusion | flops 1610612736 | bytes 16252928 | tf_op jit(solution)/shard_map/nxcd,xdf->nxcf/dot_general | solution.py:133
  145.7 7.8 %fusion.25 = bf16[4,8,48,256]{3,2,0,1:T(8,128)(2,1)S(1)} fusion(f32[8,4,48,256]{3,2,1,0:T(8,128)S(1)} %fusion.16, bf16[8,2048,256]{2,1,0:T(8,128)(2,1)} %param.30, bf16[4,8,48,2048]{3,1,0,2:T(8,128)(2,1)S(1)} %copy-done.11), kind=kOutput, calls=%fused_computation.43 | convolution fusion | flops 1612972032 | bytes 17039360 | tf_op jit(solution)/shard_map/nxcd,xdf->nxcf/dot_general | solution.py:136
  153.5 4.4 %convert_bitcast_fusion = bf16[4,8,48,2048]{3,2,0,1:T(8,128)(2,1)} fusion(bf16[4,8,48,256]{3,2,0,1:T(8,128)(2,1)S(1)} %fusion.25, bf16[8,256,2048]{2,1,0:T(8,128)(2,1)S(1)} %bitcast.110), kind=kOutput, calls=%fused_computation.32 | convolution fusion | flops 1613758464 | bytes 15466496 | tf_op jit(solution)/shard_map/nxcf,xfd->nxcd/dot_general | solution.py:138
  158.0 0.3 reduce-scatter.3.cloned.1.call-start
  158.2 0.6 copy-done.4
  159.4 7.2 %all-gather.3.cloned.1.call-done = bf16[2048,256]{1,0:T(8,128)(2,1)} async-done(((bf16[512,256]{1,0:T(8,128)(2,1)}), bf16[2048,256]{1,0:T(8,128)(2,1)}) %all-gather.3.cloned.1.call-update) | async-done | bytes 1048592 | tf_op jit(solution)/shard_map/all_gather | solution.py:84
  166.6 0.9 broadcast_in_dim.52
  167.5 4.8 %while.18 = (s32[]{:T(128)}, f32[512,1,2]{0,2,1:T(2,128)S(1)}, f32[512,1,2]{0,2,1:T(2,128)S(1)}, f32[512,1,2,128]{0,3,2,1:T(8,128)}, s32[]{:T(128)}, /*index=5*/...) while((s32[]{:T(128)}, f32[512,1,2]{0,2,1:T(2,128)S(1)}, ...), condition=%wide.region_7.8_spmd.clone, body=%wide.region_2.7_spmd.clone.sunk | while | flops 273682432 | bytes 8483165 | solution.py:100
  167.5 4.6 %conditional.3 = ((f32[512,1,2]{0,2,1:T(2,128)S(1)}, f32[512,1,2]{0,2,1:T(2,128)S(1)}, f32[512,1,2,128]{0,3,2,1:T(8,128)})) conditional(s32[]{:T(128)} %convert_element_type.128, (f32[512,1,2]{0,2,1:T(2,128)S(1)}, f32[512,1,2]{0,2,1:T(2,128)S(1)}, f32[512,1,2,128]{0,3,2,1:T(8,128)}) %tuple.58, (s32[]{:T(128)}, s32[]{:T(128)}, ...), branch_computations={%region_3.0_spmd, %region_4.6_spmd} | conditional | flops 273682432 | bytes 8480870 | solution.py:98
  167.5 0.2 broadcast_compare_fusion
  167.7 1.6 fusion.47
  169.4 2.4 fusion.5
  171.8 0.3 fusion.4
  172.3 1.1 divide_convert_fusion
  173.4 2.2 convolution_convert_fusion
  175.6 50.9 %reduce-scatter.5.cloned.1.call-done = bf16[4,8,48,512]{3,2,0,1:T(8,128)(2,1)} async-done(((bf16[4,8,48,2048]{3,2,0,1:T(8,128)(2,1)}), bf16[4,8,48,512]{3,2,0,1:T(8,128)(2,1)}) %reduce-scatter.5.cloned.1.call-update) | async-done | bytes 1572880 | tf_op jit(solution)/shard_map/reduce_scatter | solution.py:141
  226.4 2.7 copy.40
  229.1 4.7 %all-to-all-start.1 = ((bf16[4,8,48,512]{3,2,1,0:T(8,128)(2,1)}), bf16[4,8,48,512]{3,2,1,0:T(8,128)(2,1)S(1)}, u32[]{:S(2)}, u32[]{:S(2)}) async-start(bf16[4,8,48,512]{3,2,1,0:T(8,128)(2,1)} %copy.40), calls=%async_computation.3 | async-start | bytes 3145728 | tf_op jit(solution)/shard_map/all_to_all | solution.py:144
  234.2 36.5 %all-to-all-done.1 = bf16[4,8,48,512]{3,2,1,0:T(8,128)(2,1)S(1)} async-done(((bf16[4,8,48,512]{3,2,1,0:T(8,128)(2,1)}), bf16[4,8,48,512]{3,2,1,0:T(8,128)(2,1)S(1)}, u32[]{:S(2)}, u32[]{:S(2)}) %all-to-all-start.1) | async-done | bytes 1572896 | tf_op jit(solution)/shard_map/all_to_all | solution.py:144
  270.6 5.0 %gather_fusion.1 = bf16[1024,512]{1,0:T(8,128)(2,1)} fusion(bf16[1536,512]{1,0:T(8,128)(2,1)S(1)} %bitcast.108, s32[1024]{0:T(1024)S(1)} %broadcast_clamp_fusion), kind=kCustom, calls=%fused_computation.1 | custom fusion | bytes 2101248 | tf_op jit(solution)/shard_map/gather | solution.py:146
  275.7 2.4 reshape.267
  278.1 4.0 %multiply_reduce_fusion = bf16[512,512]{1,0:T(8,128)(2,1)} fusion(f32[512,2,512]{2,1,0:T(2,128)S(1)} %reshape.267, f32[512,2]{1,0:T(8,128)S(1)} %copy.41), kind=kLoop, calls=%fused_computation.41 | loop fusion | flops 786432 | bytes 2625536 | tf_op jit(solution)/shard_map/reduce_sum | solution.py:147
  (69 shorter events, 1.8 us)
Async XLA Ops:
  7.2 166.2 %copy-start = (bf16[256,2048]{1,0:T(8,128)(2,1)S(1)}, bf16[256,2048]{1,0:T(8,128)(2,1)}, u32[]{:S(2)}) copy-start(bf16[256,2048]{1,0:T(8,128)(2,1)} %param.24) | copy-start | bytes 3145732
  7.2 31.5 %copy-start.1 = (bf16[512,2048]{1,0:T(8,128)(2,1)S(1)}, bf16[512,2048]{1,0:T(8,128)(2,1)}, u32[]{:S(2)}) copy-start(bf16[512,2048]{1,0:T(8,128)(2,1)} %param.25) | copy-start | bytes 6291460
  7.2 129.2 %all-gather.5.cloned.1.call-start = ((), (), s32[]{:S(2)}) async-start(), calls=%async_computation.6 | async-start | bytes 7864320 | tf_op jit(solution)/shard_map/all_gather | solution.py:132
  29.4 9.8 %copy-start.7 = (f32[2048]{0:T(1024)S(1)}, f32[2048]{0:T(1024)}, u32[]{:S(2)}) copy-start(f32[2048]{0:T(1024)} %param.26) | copy-start | bytes 24580
  89.5 1.3 copy-start.3
  89.5 1.5 copy-start.9
  89.5 1.6 copy-start.5
  90.8 75.8 %all-gather.3.cloned.1.call-start = ((), (), s32[]{:S(2)}) async-start(), calls=%async_computation.4 | async-start | bytes 1310720 | tf_op jit(solution)/shard_map/all_gather | solution.py:84
  91.9 134.5 %reduce-scatter.5.cloned.1.call-start = ((), (), s32[]{:S(2)}) async-start(), calls=%async_computation.7 | async-start | bytes 7864320 | tf_op jit(solution)/shard_map/reduce_scatter | solution.py:141
  136.4 9.3 %copy-start.11 = (bf16[4,8,48,2048]{3,1,0,2:T(8,128)(2,1)S(1)}, bf16[4,8,48,2048]{3,1,0,2:T(8,128)(2,1)}, u32[]{:S(2)}) copy-start(bf16[4,8,48,2048]{3,1,0,2:T(8,128)(2,1)} %all-gather.5.cloned.1.call-done) | copy-start | bytes 18874372
  136.4 17.0 %slice-start = ((s8[8388608]{0:T(1024)(128)(4,1)}), s8[4194304]{0:T(1024)(128)(4,1)S(1)}, s32[]{:S(2)}) async-start(s8[8388608]{0:T(1024)(128)(4,1)} %bitcast.109), calls=%async_computation.8 | async-start | bytes 8388608
  145.7 7.8 %slice-start.1 = ((s8[8388608]{0:T(1024)(128)(4,1)}), s8[4194304]{0:T(1024)(128)(4,1)S(1)}, s32[]{:S(2)}) async-start(s8[8388608]{0:T(1024)(128)(4,1)} %bitcast.109), calls=%async_computation.9 | async-start | bytes 8388608
  157.9 1.0 copy-start.4
  157.9 1.2 copy-start.10
  157.9 1.5 copy-start.6
  158.0 124.2 %reduce-scatter.3.cloned.1.call-start = ((), (), s32[]{:S(2)}) async-start(), calls=%async_computation.5 | async-start | bytes 2621440 | tf_op jit(solution)/shard_map/reduce_scatter | solution.py:106
  229.1 4.7 %copy-start.2 = (s32[512,2]{1,0:T(8,128)S(1)}, s32[512,2]{1,0:T(8,128)}, u32[]{:S(2)}) copy-start(s32[512,2]{1,0:T(8,128)} %get-tuple-element.349) | copy-start | bytes 12292
  229.1 4.9 %copy-start.8 = (f32[2,512]{1,0:T(2,128)S(1)}, f32[2,512]{1,0:T(2,128)}, u32[]{:S(2)}) copy-start(f32[2,512]{1,0:T(2,128)} %param.28) | copy-start | bytes 12292
  229.1 41.5 %all-to-all-start.1 = ((bf16[4,8,48,512]{3,2,1,0:T(8,128)(2,1)}), bf16[4,8,48,512]{3,2,1,0:T(8,128)(2,1)S(1)}, u32[]{:S(2)}, u32[]{:S(2)}) async-start(bf16[4,8,48,512]{3,2,1,0:T(8,128)(2,1)} %copy.40), calls=%async_computation.3 | async-start | bytes 3145728 | tf_op jit(solution)/shard_map/all_to_all | solution.py:144
Sparse Core Ops, SparseCore 0:
  90.9 45.4 all-gather.4
  138.6 27.9 all-gather.2
  169.1 57.2 reduce-scatter.4
  229.4 31.1 reduce-scatter.2
where the time goes:
time: 290 us; the launch traced here: 289 us
  waiting for transfers between devices  139 us (48%)
  blocking collectives  43.1 us (15%)
  local copies, waits for them, and re-layouts  31.9 us (11%)
  other arithmetic  27.6 us (10%)
  matrix products  27.6 us (10%)
  between operations  14.1 us (5%)
  starting transfers between devices  5.3 us (2%)
    reduce_scatter x1, waiting for transfers between devices, experts_half(): lax.psum_scatter(partial_out.astype(jnp.bfloat16), 'tp', scatter_dimensio...  50.9 us
    all_gather x1, waiting for transfers between devices, experts_half(): slot_rows = lax.all_gather(arrived, 'tp', axis=2, tiled=True)  44.3 us
    all_to_all x1, blocking collectives, experts_half(): lax.all_to_all(send_rows, 'ep', split_axis=0, concat_axis=0, tiled=True)  43.1 us
    all_to_all x1, waiting for transfers between devices, experts_half(): lax.all_to_all(summed, 'ep', split_axis=0, concat_axis=0, tiled=True)  36.5 us
    another operation x2, other arithmetic  15.7 us
    dot_general x1, matrix products, experts_half(): jnp.einsum('nxcd,xdf->nxcf', slot_rows, gate_weight, preferred_element_ty...  9.27 us
    dot_general x1, matrix products, experts_half(): jnp.einsum('nxcd,xdf->nxcf', slot_rows, up_weight, preferred_element_type...  7.76 us
    all_gather x1, waiting for transfers between devices, mixer_half(): kv_piece = lax.all_gather(key_value, 'ep', axis=0, tiled=True)  7.17 us
  transfers between devices with their start and end apart: 5, of which 4 were waited for; matrix products, arithmetic and copies ran while one was open for 16% of the time, Pallas kernels for 0%

commit v1 on v0

--- a/solution.py
+++ b/solution.py
@@ -6,6 +6,8 @@
 HEAD_SIZE = 128
 EXPERTS = 32
 TOP = 2
+GROUP_SIZE = 8
+META = 128
 
 
 def head_norm(inputs, scale_gain):
@@ -146,6 +148,101 @@
     picked = result_table[slot_index]
     combined = jnp.sum(picked.astype(jnp.float32) * route_weight.T[..., None], axis=1)
     return combined.astype(jnp.bfloat16)
+
+def route_plan(routes, route_weight, n_dest, exp_dev, row_cap):
+    span_rows = routes.shape[1]
+    picks = routes[:, :, None] == jnp.arange(EXPERTS, dtype=jnp.int32)
+    dest = routes[0] // exp_dev
+    to_dest = dest[:, None] == jnp.arange(n_dest, dtype=jnp.int32)
+    marks = jnp.concatenate([picks[0] | picks[1], to_dest], axis=1).astype(jnp.bfloat16)
+    tokens = jnp.arange(span_rows, dtype=jnp.int32)
+    earlier = (tokens[None, :] < tokens[:, None]).astype(jnp.bfloat16)
+    ahead = jnp.dot(earlier, marks, preferred_element_type=jnp.float32)
+    rank = jnp.sum(jnp.where(to_dest, ahead[:, EXPERTS:], 0.0), axis=1)
+    columns = []
+    for j in range(TOP):
+        within = jnp.sum(jnp.where(picks[j], ahead[:, :EXPERTS], 0.0), axis=1)
+        columns += [(routes[j] % exp_dev + 1).astype(jnp.float32), within]
+    for j in range(TOP):
+        high = lax.reduce_precision(route_weight[j], 8, 7)
+        columns += [high, route_weight[j] - high]
+    meta = jnp.pad(jnp.stack(columns, axis=1), ((0, 0), (0, META - len(columns))))
+    return dest * row_cap + rank.astype(jnp.int32), meta.astype(jnp.bfloat16)
+
+
+def spread_rows(send_rows):
+    arrived = lax.all_to_all(send_rows, "ep", split_axis=0, concat_axis=0, tiled=True)
+    return lax.all_gather(arrived, "tp", axis=1, tiled=True)
+
+
+def return_rows(partial_rows):
+    summed = lax.psum_scatter(partial_rows, "tp", scatter_dimension=2, tiled=True)
+    return lax.all_to_all(summed, "ep", split_axis=0, concat_axis=0, tiled=True)
+
+
+def grouped_experts_half(
+    expert_rows, expert_gain, routes, route_weight, gate_weight, up_weight, down_weight
+):
+    n_tp = lax.axis_size("tp")
+    n_ep = lax.axis_size("ep")
+    span_rows, model_width = expert_rows.shape
+    exp_dev = gate_weight.shape[0]
+    capacity = n_tp * ((3 * (span_rows // n_tp) * TOP + 2 * EXPERTS - 1) // (2 * EXPERTS))
+    row_cap = exp_dev * capacity // TOP
+    part_len = row_cap // n_tp
+    row_of, meta = route_plan(routes, route_weight, n_ep, exp_dev, row_cap)
+    normed = head_norm(expert_rows, expert_gain).astype(jnp.bfloat16)
+    wanted = jnp.arange(n_ep, dtype=jnp.int32)[:, None] * row_cap + (
+        lax.axis_index("tp") * part_len + jnp.arange(part_len, dtype=jnp.int32)
+    )
+    select = (wanted.reshape(-1)[:, None] == row_of[None, :]).astype(jnp.bfloat16)
+    send_rows = jnp.dot(
+        select, jnp.concatenate([normed, meta], axis=1), preferred_element_type=jnp.float32
+    ).astype(jnp.bfloat16)
+    arrived = spread_rows(send_rows.reshape(n_ep, part_len, model_width + META))
+    notes = arrived[:, :, model_width : model_width + 8].astype(jnp.float32)
+    slots = jnp.arange(exp_dev * capacity, dtype=jnp.float32)
+    hits = []
+    for j in range(TOP):
+        local = notes[:, :, 2 * j]
+        slot = jnp.where(local > 0, (local - 1) * capacity + notes[:, :, 2 * j + 1], -1.0)
+        hits.append(slot[:, :, None] == slots)
+    slot_rows = jnp.einsum(
+        "nrq,nrd->nqd",
+        (hits[0] | hits[1]).astype(jnp.bfloat16),
+        arrived[:, :, :model_width],
+        preferred_element_type=jnp.float32,
+    ).astype(jnp.bfloat16)
+    slot_rows = slot_rows.reshape(n_ep, exp_dev, capacity, model_width)
+    gate_part = jnp.einsum(
+        "nxcd,xdf->nxcf", slot_rows, gate_weight, preferred_element_type=jnp.float32
+    )
+    up_part = jnp.einsum("nxcd,xdf->nxcf", slot_rows, up_weight, preferred_element_type=jnp.float32)
+    hidden = (jax.nn.silu(gate_part) * up_part).astype(jnp.bfloat16)
+    down_part = jnp.einsum(
+        "nxcf,xfd->nxcd", hidden, down_weight, preferred_element_type=jnp.float32
+    ).astype(jnp.bfloat16)
+    down_part = down_part.reshape(n_ep, exp_dev * capacity, model_width)
+    partial_rows = 0.0
+    for piece in range(2):
+        weights = sum(
+            jnp.where(hits[j], notes[:, :, 2 * TOP + 2 * j + piece][:, :, None], 0.0)
+            for j in range(TOP)
+        )
+        partial_rows = partial_rows + jnp.einsum(
+            "nrq,nqd->nrd",
+            weights.astype(jnp.bfloat16),
+            down_part,
+            preferred_element_type=jnp.float32,
+        )
+    returned = return_rows(partial_rows.astype(jnp.bfloat16))
+    returned = returned.reshape(n_ep * row_cap, model_width // n_tp)
+    all_rows = jnp.arange(n_ep * row_cap, dtype=jnp.int32)
+    return jnp.dot(
+        (row_of[:, None] == all_rows[None, :]).astype(jnp.bfloat16),
+        returned,
+        preferred_element_type=jnp.float32,
+    ).astype(jnp.bfloat16)
 
 
 def on_device(
@@ -167,7 +264,9 @@
     mixer_out = mixer_half(
         queries, key_rows, value_rows, query_gain, key_gain, log_forget, out_weight
     )
-    expert_out = experts_half(
+    whole_groups = gate_weight.shape[0] % GROUP_SIZE == 0
+    run_experts = grouped_experts_half if whole_groups else experts_half
+    expert_out = run_experts(
         expert_rows, expert_gain, routes, route_weight, gate_weight, up_weight, down_weight
     )
     return (mixer_out, expert_out)

time: 290 us -> 187 us (0.64)
  waiting for transfers between devices: 139 us -> 83 us
  local copies, waits for them, and re-layouts: 31.9 us -> 9.04 us
  other arithmetic: 27.6 us -> 11.5 us
  blocking collectives: 43.1 us -> 27.5 us
  matrix products: 27.6 us -> 35.5 us
    reduce_scatter x1, waiting for transfers between devices: 50.9 us -> 27.3 us  [return_rows(): lax.psum_scatter(partial_rows, 'tp', scatter_dimension=2, tiled=True)]
    all_gather x1, waiting for transfers between devices: 44.3 us -> 27.5 us  [spread_rows(): return lax.all_gather(arrived, 'tp', axis=1, tiled=True)]
    all_to_all x1, waiting for transfers between devices: 36.5 us -> 19.9 us  [return_rows(): return lax.all_to_all(summed, 'ep', split_axis=0, concat_axis=0, tiled=True)]
    all_to_all x1, blocking collectives: 43.1 us -> 27.5 us  [spread_rows(): lax.all_to_all(send_rows, 'ep', split_axis=0, concat_axis=0, tiled=True)]
    another operation x2, other arithmetic: 15.7 us -> 1.56 us
    gather x2 -> x0, local copies, waits for them, and re-layouts: 8.17 us -> none  [the longest x1 5.05 us: experts_half(): picked = result_table[slot_index]]
    reduce_scatter x1, waiting for transfers between devices: 0.01 us -> 8.17 us  [mixer_half(): lax.psum_scatter(jnp.dot(attended, out_weight, preferred_element_type=jnp...]
    dot_general x3 -> x8, matrix products: 21.4 us -> 29.3 us  [the longest x1 14 us: grouped_experts_half(): jnp.einsum('nxcf,xfd->nxcd', hidden, down_weight, preferred_element_type=...]
  transfers between devices with their start and end apart: 5 -> 5, of which waited for: 4 -> 4; matrix products, arithmetic and copies ran while one was open for 16% -> 24% of each run, Pallas kernels for 0% -> 0%
where the time goes in v1:
time: 187 us; the launch traced here: 186 us
  waiting for transfers between devices  83 us (44%)
  matrix products  35.5 us (19%)
  blocking collectives  27.5 us (15%)
  between operations  14.1 us (8%)
  other arithmetic  11.5 us (6%)
  local copies, waits for them, and re-layouts  9.04 us (5%)
  starting transfers between devices  5.17 us (3%)
    all_to_all x1, blocking collectives, spread_rows(): lax.all_to_all(send_rows, 'ep', split_axis=0, concat_axis=0, tiled=True)  27.5 us
    all_gather x1, waiting for transfers between devices, spread_rows(): return lax.all_gather(arrived, 'tp', axis=1, tiled=True)  27.5 us
    reduce_scatter x1, waiting for transfers between devices, return_rows(): lax.psum_scatter(partial_rows, 'tp', scatter_dimension=2, tiled=True)  27.3 us
    all_to_all x1, waiting for transfers between devices, return_rows(): return lax.all_to_all(summed, 'ep', split_axis=0, concat_axis=0, tiled=True)  19.9 us
    dot_general x1, matrix products, grouped_experts_half(): jnp.einsum('nxcf,xfd->nxcd', hidden, down_weight, preferred_element_type=...  14 us
    reduce_scatter x1, waiting for transfers between devices, mixer_half(): lax.psum_scatter(jnp.dot(attended, out_weight, preferred_element_type=jnp...  8.17 us
    dot_general x1, matrix products, grouped_experts_half(): jnp.einsum('nxcd,xdf->nxcf', slot_rows, gate_weight, preferred_element_ty...  5.54 us
    dot_general x2, matrix products, grouped_experts_half(): jnp.einsum('nrq,nqd->nrd', weights.astype(jnp.bfloat16), down_part, prefe...  5.48 us
  transfers between devices with their start and end apart: 5, of which 4 were waited for; matrix products, arithmetic and copies ran while one was open for 24% of the time, Pallas kernels for 0%

profile of v1, /device:TPU:0, one launch (start us, length us, event | category | flops | bytes accessed | tf_op | source)
XLA Modules:
  0.0 186.0 jit_solution(6827125404856298380)
XLA Ops:
  7.2 0.8 slice.70
  8.1 0.7 iota_compare_fusion.9
  8.8 0.8 fusion.91
  9.7 0.2 fusion.49
  9.9 0.1 select_reduce_fusion
  10.0 0.8 fusion.84
  10.9 0.2 copy.32
  11.0 0.7 multiply_add_fusion
  11.8 0.1 broadcast_add_fusion.1
  11.8 0.1 add.249
  11.9 2.1 %fusion.23 = f32[512]{0:T(512)S(1)} fusion(bf16[512,2048]{1,0:T(8,128)(2,1)} %param.25), kind=kLoop, calls=%fused_computation.38 | loop fusion | flops 3145216 | bytes 2099200 | tf_op jit(solution)/shard_map/reduce_sum | solution.py:15
  14.0 0.6 fusion.25
  14.6 0.7 convolution_convert_fusion.1
  15.3 27.5 %all_to_all.10 = bf16[4,48,2176]{2,1,0:T(8,128)(2,1)} all-to-all(bf16[4,48,2176]{2,1,0:T(8,128)(2,1)S(1)} %bitcast.131), channel_id=1, replica_groups=mesh['grp'=2,'ep'=4,'tp'=4] {'ep'}, dimensions={0} | all-to-all | bytes 1671168 | tf_op jit(solution)/shard_map/all_to_all | solution.py:174
  42.9 0.1 fusion.73
  43.1 0.1 fusion.75
  43.3 0.7 pad_maximum_fusion
  44.0 0.2 reduce-scatter.5.cloned.1.call-start
  44.3 27.5 %all-gather.5.cloned.1.call-done = bf16[4,192,2176]{2,1,0:T(8,128)(2,1)} async-done(((bf16[4,48,2176]{2,1,0:T(8,128)(2,1)}), bf16[4,192,2176]{2,1,0:T(8,128)(2,1)}) %all-gather.5.cloned.1.call-update) | async-done | bytes 3342352 | tf_op jit(solution)/shard_map/all_gather | solution.py:175
  71.8 1.1 slice_convert_fusion
  72.9 1.6 slice_reduce_fusion.1
  74.5 2.0 %convolution_convert_fusion = bf16[4,384,2048]{2,1,0:T(8,128)(2,1)S(1)} fusion(bf16[4,192,2176]{2,1,0:T(8,128)(2,1)S(1)} %copy-done.3, f32[4,192]{1,0:T(4,128)S(1)} %get-tuple-element.315, f32[4,192]{1,0:T(4,128)S(1)} %get-tuple-element.318), kind=kOutput, calls=%fused_computation.35 | convolution fusion | flops 1211990016 | bytes 9445376 | tf_op jit(solution)/shard_map/nrq,nrd->nqd/dot_general | solution.py:210
  76.5 2.7 %copy-done.2 = bf16[4,384,2048]{2,1,0:T(8,128)(2,1)} copy-done((bf16[4,384,2048]{2,1,0:T(8,128)(2,1)}, bf16[4,384,2048]{2,1,0:T(8,128)(2,1)S(1)}, u32[]{:S(2)}) %copy-start.2) | copy-done | bytes 6291480
  79.1 5.5 %fusion.16 = f32[8,4,48,256]{3,2,1,0:T(8,128)S(1)} fusion(bf16[8,2048,256]{2,1,0:T(8,128)(2,1)} %param.29, bf16[4,8,48,2048]{3,2,1,0:T(8,128)(2,1)S(1)} %bitcast.125), kind=kOutput, calls=%fused_computation.27 | convolution fusion | flops 1610612736 | bytes 16252928 | tf_op jit(solution)/shard_map/nxcd,xdf->nxcf/dot_general | solution.py:217
  84.7 14.0 %convert_bitcast_fusion = bf16[4,8,48,2048]{3,2,0,1:T(8,128)(2,1)} fusion(bf16[8,256,2048]{2,1,0:T(8,128)(2,1)} %param.31, f32[8,4,48,256]{3,2,1,0:T(8,128)S(1)} %fusion.16, bf16[8,2048,256]{2,1,0:T(8,128)(2,1)} %param.30, bf16[4,8,48,2048]{3,2,1,0:T(8,128)(2,1)} %bitcast.126), kind=kOutput, calls=%fused_computation.30 | convolution fusion | flops 3226730496 | bytes 30932992 | tf_op jit(solution)/shard_map/nxcf,xfd->nxcd/dot_general | solution.py:222
  98.7 3.4 %copy.25 = bf16[4,8,48,2048]{3,2,1,0:T(8,128)(2,1)S(1)} copy(bf16[4,8,48,2048]{3,2,0,1:T(8,128)(2,1)} %convert_bitcast_fusion) | data formatting | bytes 12582912 | tf_op jit(solution)/shard_map/convert_element_type | solution.py:224
  102.0 1.9 %fusion.52 = f32[4,192,2048]{2,1,0:T(8,128)S(1)} fusion(bf16[4,384,2048]{2,1,0:T(8,128)(2,1)S(1)} %bitcast.123, f32[4,192]{1,0:T(4,128)S(1)} %get-tuple-element.314, f32[4,192]{1,0:T(4,128)S(1)} %get-tuple-element.315, f32[4,192]{1,0:T(4,128)S(1)} %get-tuple-element.317, f32[4,192]{1,0:T(4,128)S(1)} %get-tuple-element.318), kind=kOutput, calls=%fused_computation.70 | convolution fusion | flops 1209729024 | bytes 12595200 | tf_op jit(solution)/shard_map/nrq,nqd->nrd/dot_general | solution.py:232
  103.9 3.6 %add_convert_fusion = bf16[4,192,2048]{2,1,0:T(8,128)(2,1)} fusion(f32[4,192,2048]{2,1,0:T(8,128)S(1)} %fusion.52, bf16[4,384,2048]{2,1,0:T(8,128)(2,1)S(1)} %bitcast.124, f32[4,192]{1,0:T(4,128)S(1)} %get-tuple-element.316, f32[4,192]{1,0:T(4,128)S(1)} %get-tuple-element.313, f32[4,192]{1,0:T(4,128)S(1)} %get-tuple-element.315, ...), kind=kOutput, calls=%fused_computation.29 | convolution fusion | flops 1212874752 | bytes 15740928 | tf_op jit(solution)/shard_map/nrq,nqd->nrd/dot_general | solution.py:232
  107.5 0.3 reduce-scatter.3.cloned.1.call-start
  107.8 0.6 copy-done.5
  108.5 0.1 copy.21
  108.6 0.1 fusion.65
  108.7 0.1 fusion.67
  108.8 0.2 copy.22
  109.0 0.9 broadcast_in_dim.104
  109.9 4.9 %while.18 = (s32[]{:T(128)}, f32[512,1,2]{0,2,1:T(2,128)S(1)}, f32[512,1,2]{0,2,1:T(2,128)S(1)}, f32[512,1,2,128]{0,3,2,1:T(8,128)}, s32[]{:T(128)}, /*index=5*/...) while((s32[]{:T(128)}, f32[512,1,2]{0,2,1:T(2,128)S(1)}, ...), condition=%wide.region_7.8_spmd.clone, body=%wide.region_2.7_spmd.clone.sunk | while | flops 273682432 | bytes 8483165 | solution.py:102
  109.9 4.7 %conditional.3 = ((f32[512,1,2]{0,2,1:T(2,128)S(1)}, f32[512,1,2]{0,2,1:T(2,128)S(1)}, f32[512,1,2,128]{0,3,2,1:T(8,128)})) conditional(s32[]{:T(128)} %convert_element_type.207, (f32[512,1,2]{0,2,1:T(2,128)S(1)}, f32[512,1,2]{0,2,1:T(2,128)S(1)}, f32[512,1,2,128]{0,3,2,1:T(8,128)}) %tuple.66, (s32[]{:T(128)}, s32[]{:T(128)}, ...), branch_computations={%region_3.0_spmd, %region_4.6_spmd} | conditional | flops 273682432 | bytes 8480870 | solution.py:100
  110.0 0.2 broadcast_compare_fusion
  110.2 1.6 fusion.102
  111.8 2.5 %fusion.5 = f32[512,1,2,128]{0,3,2,1:T(8,128)} fusion(f32[512,1,2,512]{0,3,2,1:T(8,128)S(1)} %get-tuple-element.344, f32[512,2]{0,1:T(2,128)S(1)} %bitcast.127, f32[512,1,2,128]{0,3,2,1:T(8,128)} %get-tuple-element.253, f32[512,2]{0,1:T(2,128)S(1)} %get-tuple-element.341, bf16[2048,256]{1,0:T(8,128)(2,1)} %get-tuple-element.248, s32[]{:T(128)S(6)} %select_n.80, ...), kind=kOutput, calls=%fused_computation.8 | convolution fusion | flops 135528448 | bytes 3285000 | tf_op jit(solution)/shard_map/while/body/eval_jaxpr/cond/branch_1_fun/qgrk,kgd->qgrd/dot_general | solution.py:73
  114.3 0.3 fusion.4
  114.8 1.2 divide_convert_fusion
  115.9 2.1 %convolution_convert_fusion.2 = bf16[512,2048]{1,0:T(8,128)(2,1)} fusion(bf16[512,256]{0,1:T(8,128)(2,1)S(1)} %bitcast.130, bf16[256,2048]{1,0:T(8,128)(2,1)S(1)} %copy-done), kind=kOutput, calls=%fused_computation.43 | convolution fusion | flops 537919488 | bytes 3407872 | tf_op jit(solution)/shard_map/dot_general | solution.py:109
  118.1 27.3 %reduce-scatter.5.cloned.1.call-done = bf16[4,192,512]{2,1,0:T(8,128)(2,1)} async-done(((bf16[4,192,2048]{2,1,0:T(8,128)(2,1)}), bf16[4,192,512]{2,1,0:T(8,128)(2,1)}) %reduce-scatter.5.cloned.1.call-update) | async-done | bytes 786448 | tf_op jit(solution)/shard_map/reduce_scatter | solution.py:179
  145.4 4.6 %all-to-all-start.1 = ((bf16[4,192,512]{2,1,0:T(8,128)(2,1)}), bf16[4,192,512]{2,1,0:T(8,128)(2,1)S(1)}, u32[]{:S(2)}, u32[]{:S(2)}) async-start(bf16[4,192,512]{2,1,0:T(8,128)(2,1)} %reduce-scatter.5.cloned.1.call-done), calls=%async_computation.3 | async-start | bytes 1572864 | tf_op jit(solution)/shard_map/all_to_all | solution.py:180
  150.0 19.9 %all-to-all-done.1 = bf16[4,192,512]{2,1,0:T(8,128)(2,1)S(1)} async-done(((bf16[4,192,512]{2,1,0:T(8,128)(2,1)}), bf16[4,192,512]{2,1,0:T(8,128)(2,1)S(1)}, u32[]{:S(2)}, u32[]{:S(2)}) %all-to-all-start.1) | async-done | bytes 786464 | tf_op jit(solution)/shard_map/all_to_all | solution.py:180
  169.9 1.4 fusion.45
  171.3 8.2 %reduce-scatter.3.cloned.1.call-done = bf16[128,2048]{1,0:T(8,128)(2,1)} async-done(((bf16[512,2048]{1,0:T(8,128)(2,1)}), bf16[128,2048]{1,0:T(8,128)(2,1)}) %reduce-scatter.3.cloned.1.call-update) | async-done | bytes 524304 | tf_op jit(solution)/shard_map/reduce_scatter | solution.py:108
  (56 shorter events, 0.5 us)
Async XLA Ops:
  7.2 108.8 %copy-start = (bf16[256,2048]{1,0:T(8,128)(2,1)S(1)}, bf16[256,2048]{1,0:T(8,128)(2,1)}, u32[]{:S(2)}) copy-start(bf16[256,2048]{1,0:T(8,128)(2,1)} %param.24) | copy-start | bytes 3145732
  7.2 6.8 %copy-start.1 = (bf16[512,2048]{1,0:T(8,128)(2,1)S(1)}, bf16[512,2048]{1,0:T(8,128)(2,1)}, u32[]{:S(2)}) copy-start(bf16[512,2048]{1,0:T(8,128)(2,1)} %param.25) | copy-start | bytes 6291460
  7.2 6.8 %copy-start.8 = (f32[2048]{0:T(1024)S(1)}, f32[2048]{0:T(1024)}, u32[]{:S(2)}) copy-start(f32[2048]{0:T(1024)} %param.26) | copy-start | bytes 24580
  7.2 64.6 %all-gather.5.cloned.1.call-start = ((), (), s32[]{:S(2)}) async-start(), calls=%async_computation.6 | async-start | bytes 4177920 | tf_op jit(solution)/shard_map/all_gather | solution.py:175
  15.3 27.6 %copy-start.4 = (bf16[512,128]{1,0:T(8,128)(2,1)S(1)}, bf16[512,128]{1,0:T(8,128)(2,1)}, u32[]{:S(2)}) copy-start(bf16[512,128]{1,0:T(8,128)(2,1)} %param.19) | copy-start | bytes 393220
  15.3 27.8 %copy-start.9 = (f32[128]{0:T(128)S(1)}, f32[128]{0:T(128)}, u32[]{:S(2)}) copy-start(f32[128]{0:T(128)} %param.22) | copy-start | bytes 1540
  15.3 27.9 %copy-start.6 = (bf16[512,128]{1,0:T(8,128)(2,1)S(1)}, bf16[512,128]{1,0:T(8,128)(2,1)}, u32[]{:S(2)}) copy-start(bf16[512,128]{1,0:T(8,128)(2,1)} %param.20) | copy-start | bytes 393220
  42.9 66.2 %all-gather.3.cloned.1.call-start = ((), (), s32[]{:S(2)}) async-start(), calls=%async_computation.4 | async-start | bytes 1310720 | tf_op jit(solution)/shard_map/all_gather | solution.py:86
  44.0 101.3 %reduce-scatter.5.cloned.1.call-start = ((), (), s32[]{:S(2)}) async-start(), calls=%async_computation.7 | async-start | bytes 3932160 | tf_op jit(solution)/shard_map/reduce_scatter | solution.py:179
  71.8 2.8 %copy-start.3 = (bf16[4,192,2176]{2,1,0:T(8,128)(2,1)S(1)}, bf16[4,192,2176]{2,1,0:T(8,128)(2,1)}, u32[]{:S(2)}) copy-start(bf16[4,192,2176]{2,1,0:T(8,128)(2,1)} %all-gather.5.cloned.1.call-done) | copy-start | bytes 10027012
  76.5 2.7 %copy-start.2 = (bf16[4,384,2048]{2,1,0:T(8,128)(2,1)}, bf16[4,384,2048]{2,1,0:T(8,128)(2,1)S(1)}, u32[]{:S(2)}) copy-start(bf16[4,384,2048]{2,1,0:T(8,128)(2,1)S(1)} %convolution_convert_fusion) | copy-start | bytes 18874372
  107.5 0.9 copy-start.5
  107.5 1.2 copy-start.10
  107.5 1.5 copy-start.7
  107.5 72.0 %reduce-scatter.3.cloned.1.call-start = ((), (), s32[]{:S(2)}) async-start(), calls=%async_computation.5 | async-start | bytes 2621440 | tf_op jit(solution)/shard_map/reduce_scatter | solution.py:108
  145.4 24.6 %all-to-all-start.1 = ((bf16[4,192,512]{2,1,0:T(8,128)(2,1)}), bf16[4,192,512]{2,1,0:T(8,128)(2,1)S(1)}, u32[]{:S(2)}, u32[]{:S(2)}) async-start(bf16[4,192,512]{2,1,0:T(8,128)(2,1)} %reduce-scatter.5.cloned.1.call-done), calls=%async_computation.3 | async-start | bytes 1572864 | tf_op jit(solution)/shard_map/all_to_all | solution.py:180
Sparse Core Ops, SparseCore 0:
  43.0 28.7 all-gather.4
  73.9 27.9 all-gather.2
  107.7 37.6 reduce-scatter.4
  148.3 31.1 reduce-scatter.2

commit v2 on v1

--- a/solution.py
+++ b/solution.py
@@ -1,6 +1,10 @@
+import functools
+
 import jax
 import jax.numpy as jnp
 from jax import lax
+from jax.experimental import pallas as pl
+from jax.experimental.pallas import tpu as pltpu
 from jax.sharding import PartitionSpec as P
 
 HEAD_SIZE = 128
@@ -105,12 +109,7 @@
         .astype(jnp.bfloat16)
         .reshape(span_rows, heads_dev * HEAD_SIZE)
     )
-    return lax.psum_scatter(
-        jnp.dot(attended, out_weight, preferred_element_type=jnp.float32).astype(jnp.bfloat16),
-        "tp",
-        scatter_dimension=0,
-        tiled=True,
-    )
+    return jnp.dot(attended, out_weight, preferred_element_type=jnp.float32).astype(jnp.bfloat16)
 
 
 def experts_half(
@@ -170,18 +169,233 @@
     return dest * row_cap + rank.astype(jnp.int32), meta.astype(jnp.bfloat16)
 
 
+def ring_peers(n_ep, n_tp):
+    me = lax.axis_index("ep")
+    mine = lax.axis_index("tp")
+    pair = mine + 1 - 2 * (mine % 2)
+    across = (mine + n_tp // 2) % n_tp
+    return me, mine, pair, across
+
+
+def meet(me, pair, across, n_ep):
+    barrier = pltpu.get_barrier_semaphore()
+    peers = [{"ep": (me + k) % n_ep} for k in range(1, n_ep)] + [{"tp": pair}, {"tp": across}]
+    for peer in peers:
+        pl.semaphore_signal(
+            barrier, inc=1, device_id=peer, device_id_type=pl.DeviceIdType.MESH
+        )
+    pl.semaphore_wait(barrier, len(peers))
+
+
+def remote(src, dst, send_sem, recv_sem, peer):
+    return pltpu.make_async_remote_copy(
+        src_ref=src,
+        dst_ref=dst,
+        send_sem=send_sem,
+        recv_sem=recv_sem,
+        device_id=peer,
+        device_id_type=pl.DeviceIdType.MESH,
+    )
+
+
+def spread_kernel(
+    n_ep, n_tp, send_ref, out_ref, own_sem, z_send, z_recv, x_send, x_recv, c_send, c_recv
+):
+    me, mine, pair, across = ring_peers(n_ep, n_tp)
+    meet(me, pair, across, n_ep)
+    along = []
+    for k in range(1, n_ep):
+        dest = (me + k) % n_ep
+        copy = remote(
+            send_ref.at[dest], out_ref.at[me, mine], z_send.at[k], z_recv.at[k], {"ep": dest}
+        )
+        copy.start()
+        along.append(copy)
+    own = pltpu.make_async_copy(send_ref.at[me], out_ref.at[me, mine], own_sem)
+    own.start()
+    crossing = []
+    pairing = []
+
+    def pass_on(k):
+        source = (me + n_ep - k) % n_ep
+        block = send_ref.at[me] if k == 0 else out_ref.at[source, mine]
+        place = out_ref.at[source, mine]
+        copy = remote(block, place, x_send.at[k], x_recv.at[k], {"tp": across})
+        copy.start()
+        crossing.append(copy)
+        copy = remote(block, place, c_send.at[0, k], c_recv.at[0, k], {"tp": pair})
+        copy.start()
+        pairing.append(copy)
+
+    def relay(k):
+        source = (me + n_ep - k) % n_ep
+        crossing[k].wait_recv()
+        place = out_ref.at[source, across]
+        copy = remote(place, place, c_send.at[1, k], c_recv.at[1, k], {"tp": pair})
+        copy.start()
+        pairing.append(copy)
+
+    pass_on(0)
+    for k in range(1, n_ep):
+        along[k - 1].wait_recv()
+        pass_on(k)
+        relay(k - 1)
+    relay(n_ep - 1)
+    for copy in pairing:
+        copy.wait()
+    for copy in crossing + along:
+        copy.wait_send()
+    own.wait()
+
+
 def spread_rows(send_rows):
-    arrived = lax.all_to_all(send_rows, "ep", split_axis=0, concat_axis=0, tiled=True)
-    return lax.all_gather(arrived, "tp", axis=1, tiled=True)
-
-
-def return_rows(partial_rows):
-    summed = lax.psum_scatter(partial_rows, "tp", scatter_dimension=2, tiled=True)
-    return lax.all_to_all(summed, "ep", split_axis=0, concat_axis=0, tiled=True)
+    n_ep = lax.axis_size("ep")
+    n_tp = lax.axis_size("tp")
+    if n_tp != 4:
+        arrived = lax.all_to_all(send_rows, "ep", split_axis=0, concat_axis=0, tiled=True)
+        return lax.all_gather(arrived, "tp", axis=1, tiled=True)
+    _, part_len, width = send_rows.shape
+    dma = pltpu.SemaphoreType.DMA
+    arrived = pl.pallas_call(
+        functools.partial(spread_kernel, n_ep, n_tp),
+        out_shape=jax.ShapeDtypeStruct((n_ep, n_tp, part_len, width), send_rows.dtype),
+        in_specs=[pl.BlockSpec(memory_space=pltpu.VMEM)],
+        out_specs=pl.BlockSpec(memory_space=pltpu.VMEM),
+        scratch_shapes=[
+            dma,
+            dma((n_ep,)),
+            dma((n_ep,)),
+            dma((n_ep,)),
+            dma((n_ep,)),
+            dma((2, n_ep)),
+            dma((2, n_ep)),
+        ],
+        compiler_params=pltpu.CompilerParams(
+            collective_id=0, has_side_effects=True, vmem_limit_bytes=16 * 2**20
+        ),
+        cost_estimate=pl.CostEstimate(flops=0, bytes_accessed=50_000_000, transcendentals=0),
+    )(send_rows)
+    return arrived.reshape(n_ep, n_tp * part_len, width)
+
+
+def return_kernel(
+    n_ep,
+    n_tp,
+    rows_ref,
+    after_ref,
+    out_ref,
+    paired,
+    leaving,
+    crossed,
+    final,
+    c_send,
+    c_recv,
+    x_send,
+    x_recv,
+    z_send,
+    z_recv,
+):
+    me, mine, pair, across = ring_peers(n_ep, n_tp)
+    meet(me, pair, across, n_ep)
+    width = out_ref.shape[2]
+    pair_across = (pair + n_tp // 2) % n_tp
+
+    def columns(quarter):
+        return pl.ds(pl.multiple_of(quarter * width, width), width)
+
+    order = list(range(1, n_ep)) + [0]
+    pairing = {}
+    for k in order:
+        dest = (me + k) % n_ep
+        for side, quarter in ((1, pair_across), (0, pair)):
+            copy = remote(
+                rows_ref.at[dest, :, columns(quarter)],
+                paired.at[side, k],
+                c_send.at[side, k],
+                c_recv.at[side, k],
+                {"tp": pair},
+            )
+            copy.start()
+            pairing[side, k] = copy
+    crossing = {}
+    for k in order:
+        dest = (me + k) % n_ep
+        pairing[1, k].wait_recv()
+        both = rows_ref[dest, :, columns(across)].astype(jnp.float32) + paired[1, k].astype(
+            jnp.float32
+        )
+        leaving[k] = both.astype(leaving.dtype)
+        copy = remote(leaving.at[k], crossed.at[k], x_send.at[k], x_recv.at[k], {"tp": across})
+        copy.start()
+        crossing[k] = copy
+    along = []
+    for k in order:
+        dest = (me + k) % n_ep
+        pairing[0, k].wait_recv()
+        crossing[k].wait_recv()
+        total = rows_ref[dest, :, columns(mine)].astype(jnp.float32) + paired[0, k].astype(
+            jnp.float32
+        )
+        total = (total + crossed[k].astype(jnp.float32)).astype(out_ref.dtype)
+        if k == 0:
+            out_ref[me] = total
+        else:
+            final[k] = total
+            copy = remote(final.at[k], out_ref.at[me], z_send.at[k], z_recv.at[k], {"ep": dest})
+            copy.start()
+            along.append(copy)
+    for copy in along:
+        copy.wait()
+    for copy in list(pairing.values()) + list(crossing.values()):
+        copy.wait_send()
+
+
+def return_rows(partial_rows, after):
+    n_ep = lax.axis_size("ep")
+    n_tp = lax.axis_size("tp")
+    if n_tp != 4:
+        summed = lax.psum_scatter(partial_rows, "tp", scatter_dimension=2, tiled=True)
+        return lax.all_to_all(summed, "ep", split_axis=0, concat_axis=0, tiled=True)
+    _, row_cap, model_width = partial_rows.shape
+    width = model_width // n_tp
+    dma = pltpu.SemaphoreType.DMA
+    kind = partial_rows.dtype
+    return pl.pallas_call(
+        functools.partial(return_kernel, n_ep, n_tp),
+        out_shape=jax.ShapeDtypeStruct((n_ep, row_cap, width), kind),
+        in_specs=[
+            pl.BlockSpec(memory_space=pltpu.VMEM),
+            pl.BlockSpec(memory_space=pl.ANY),
+        ],
+        out_specs=pl.BlockSpec(memory_space=pltpu.VMEM),
+        scratch_shapes=[
+            pltpu.VMEM((2, n_ep, row_cap, width), kind),
+            pltpu.VMEM((n_ep, row_cap, width), kind),
+            pltpu.VMEM((n_ep, row_cap, width), kind),
+            pltpu.VMEM((n_ep, row_cap, width), kind),
+            dma((2, n_ep)),
+            dma((2, n_ep)),
+            dma((n_ep,)),
+            dma((n_ep,)),
+            dma((n_ep,)),
+            dma((n_ep,)),
+        ],
+        compiler_params=pltpu.CompilerParams(
+            collective_id=1, has_side_effects=True, vmem_limit_bytes=20 * 2**20
+        ),
+        cost_estimate=pl.CostEstimate(flops=0, bytes_accessed=50_000_000, transcendentals=0),
+    )(partial_rows, after)
 
 
 def grouped_experts_half(
-    expert_rows, expert_gain, routes, route_weight, gate_weight, up_weight, down_weight
+    expert_rows,
+    expert_gain,
+    routes,
+    route_weight,
+    gate_weight,
+    up_weight,
+    down_weight,
+    mixer_part,
 ):
     n_tp = lax.axis_size("tp")
     n_ep = lax.axis_size("ep")
@@ -200,6 +414,7 @@
         select, jnp.concatenate([normed, meta], axis=1), preferred_element_type=jnp.float32
     ).astype(jnp.bfloat16)
     arrived = spread_rows(send_rows.reshape(n_ep, part_len, model_width + META))
+    arrived, mixer_part = lax.optimization_barrier((arrived, mixer_part))
     notes = arrived[:, :, model_width : model_width + 8].astype(jnp.float32)
     slots = jnp.arange(exp_dev * capacity, dtype=jnp.float32)
     hits = []
@@ -235,7 +450,7 @@
             down_part,
             preferred_element_type=jnp.float32,
         )
-    returned = return_rows(partial_rows.astype(jnp.bfloat16))
+    returned = return_rows(partial_rows.astype(jnp.bfloat16), mixer_part[:16, :128])
     returned = returned.reshape(n_ep * row_cap, model_width // n_tp)
     all_rows = jnp.arange(n_ep * row_cap, dtype=jnp.int32)
     return jnp.dot(
@@ -261,14 +476,23 @@
     up_weight,
     down_weight,
 ):
-    mixer_out = mixer_half(
+    mixer_part = mixer_half(
         queries, key_rows, value_rows, query_gain, key_gain, log_forget, out_weight
     )
-    whole_groups = gate_weight.shape[0] % GROUP_SIZE == 0
-    run_experts = grouped_experts_half if whole_groups else experts_half
-    expert_out = run_experts(
-        expert_rows, expert_gain, routes, route_weight, gate_weight, up_weight, down_weight
-    )
+    expert_args = (
+        expert_rows,
+        expert_gain,
+        routes,
+        route_weight,
+        gate_weight,
+        up_weight,
+        down_weight,
+    )
+    if gate_weight.shape[0] % GROUP_SIZE == 0:
+        expert_out = grouped_experts_half(*expert_args, mixer_part)
+    else:
+        expert_out = experts_half(*expert_args)
+    mixer_out = lax.psum_scatter(mixer_part, "tp", scatter_dimension=0, tiled=True)
     return (mixer_out, expert_out)
 
 

time: 187 us -> 162 us (0.87)
  Pallas kernels: 0 us -> 87.4 us
  waiting for transfers between devices: 83 us -> 0.05 us
  blocking collectives: 27.5 us -> 0 us
  starting transfers between devices: 5.17 us -> 0.08 us
  other arithmetic: 11.5 us -> 15 us
  matrix products: 35.5 us -> 32.8 us
  local copies, waits for them, and re-layouts: 9.04 us -> 11.6 us
    pallas_call x0 -> x2, Pallas kernels: none -> 87.4 us  [the longest x1 44.2 us: return_rows(): pl.pallas_call(functools.partial(return_kernel, n_ep, n_tp), out_shape=ja...]
    reduce_scatter x2 -> x1, waiting for transfers between devices: 35.4 us -> 0.01 us  [on_device(): lax.psum_scatter(mixer_part, 'tp', scatter_dimension=0, tiled=True)]
    all_to_all x1 -> x0, blocking collectives: 27.5 us -> none  [spread_rows(): lax.all_to_all(send_rows, 'ep', split_axis=0, concat_axis=0, tiled=True)]
    all_gather x1 -> x0, waiting for transfers between devices: 27.5 us -> none  [spread_rows(): return lax.all_gather(arrived, 'tp', axis=1, tiled=True)]
    all_to_all x1 -> x0, waiting for transfers between devices: 19.9 us -> none  [return_rows(): return lax.all_to_all(summed, 'ep', split_axis=0, concat_axis=0, tiled=True)]
    all_to_all x1 -> x0, starting transfers between devices: 4.6 us -> none  [return_rows(): return lax.all_to_all(summed, 'ep', split_axis=0, concat_axis=0, tiled=True)]
    unnamed x25 -> x23, local copies, waits for them, and re-layouts: 3.81 us -> 6.09 us
  transfers between devices with their start and end apart: 5 -> 2, of which waited for: 4 -> 0; matrix products, arithmetic and copies ran while one was open for 24% -> 28% of each run, Pallas kernels for 0% -> 54%
where the time goes in v2:
time: 162 us
  Pallas kernels  87.4 us (54%)
  matrix products  32.8 us (20%)
  other arithmetic  15 us (9%)
  between operations  14.4 us (9%)
  local copies, waits for them, and re-layouts  11.6 us (7%)
    pallas_call x1, Pallas kernels, return_rows(): pl.pallas_call(functools.partial(return_kernel, n_ep, n_tp), out_shape=ja...  44.2 us
    pallas_call x1, Pallas kernels, spread_rows(): pl.pallas_call(functools.partial(spread_kernel, n_ep, n_tp), out_shape=ja...  43.2 us
    dot_general x1, matrix products, grouped_experts_half(): jnp.einsum('nxcf,xfd->nxcd', hidden, down_weight, preferred_element_type=...  13.9 us
    unnamed x23, local copies, waits for them, and re-layouts  6.09 us
    dot_general x1, matrix products, grouped_experts_half(): jnp.einsum('nxcd,xdf->nxcf', slot_rows, gate_weight, preferred_element_ty...  5.26 us
    dot_general x2, matrix products, grouped_experts_half(): jnp.einsum('nrq,nqd->nrd', weights.astype(jnp.bfloat16), down_part, prefe...  4.14 us
    convert_element_type x1, local copies, waits for them, and re-layouts, grouped_experts_half(): down_part = jnp.einsum('nxcf,xfd->nxcd', hidden, down_weight, preferred_e...  3.36 us
    reduce_sum x3, other arithmetic, head_norm(): jnp.mean(widened * widened, axis=-1, keepdims=True) + 1e-06  3.27 us
  transfers between devices with their start and end apart: 2, of which 0 were waited for; matrix products, arithmetic and copies ran while one was open for 28% of the time, Pallas kernels for 54%

profile of v2, /device:TPU:0, one launch (start us, length us, event | category | flops | bytes accessed | tf_op | source)
XLA Modules:
  0.0 161.8 jit_solution(12535462204321179331)
XLA Ops:
  7.2 0.0 all-gather.2.cloned.1.call-start
  7.2 1.1 fusion.73
  8.4 1.0 fusion.75
  9.4 1.6 %pad_maximum_fusion = bf16[512,256]{1,0:T(8,128)(2,1)} fusion(bf16[512,128]{1,0:T(8,128)(2,1)} %param.20, bf16[512,128]{1,0:T(8,128)(2,1)S(1)} %fusion.75), kind=kLoop, calls=%fused_computation.103 | loop fusion | flops 524288 | bytes 524288 | tf_op jit(solution)/shard_map/concatenate | solution.py:49
  11.1 0.0 all-gather.2.cloned.1.call-update
  11.1 0.0 reduce-scatter.2.cloned.1.call-start
  11.2 0.7 slice.73
  11.8 0.8 fusion.91
  12.6 0.7 iota_compare_fusion.9
  13.4 0.2 fusion.49
  13.6 0.1 select_reduce_fusion
  13.8 0.1 broadcast_add_fusion.1
  13.8 0.7 add.247
  14.5 2.1 %fusion.23 = f32[512]{0:T(512)S(1)} fusion(bf16[512,2048]{1,0:T(8,128)(2,1)} %param.25), kind=kLoop, calls=%fused_computation.38 | loop fusion | flops 3145216 | bytes 2099200 | tf_op jit(solution)/shard_map/reduce_sum | solution.py:19
  16.6 0.6 convert_element_type.143
  17.2 0.2 copy.32
  17.4 1.1 copy.21
  18.5 0.1 fusion.65
  18.6 1.5 fusion.67
  20.1 1.1 copy.22
  21.2 0.7 multiply_add_fusion
  21.9 1.2 fusion.25
  23.2 0.7 convolution_convert_fusion.1
  23.9 43.2 %shard_map.149 = bf16[4,4,48,2176]{3,2,1,0:T(8,128)(2,1)S(1)} custom-call(bf16[4,48,2176]{2,1,0:T(8,128)(2,1)S(1)} %bitcast.126), custom_call_target="tpu_custom_call" | custom-call | bytes 50000000 | tf_op jit(solution)/shard_map/pallas_call | solution.py:259
  67.1 1.7 %copy-done.2 = bf16[4,4,48,2176]{3,2,1,0:T(8,128)(2,1)} copy-done((bf16[4,4,48,2176]{3,2,1,0:T(8,128)(2,1)}, bf16[4,4,48,2176]{3,2,1,0:T(8,128)(2,1)S(1)}, u32[]{:S(2)}) %copy-start.2) | copy-done | bytes 3342360
  68.8 0.0 all-gather.2.cloned.1.call-done
  68.8 0.1 broadcast_in_dim.104
  68.9 4.1 %while.18 = (s32[]{:T(128)}, f32[512,1,2]{0,2,1:T(2,128)S(1)}, f32[512,1,2]{0,2,1:T(2,128)S(1)}, f32[512,1,2,128]{0,3,2,1:T(8,128)S(1)}, s32[]{:T(128)}, /*index...) while((s32[]{:T(128)}, f32[512,1,2]{0,2,1:T(2,128)S(1)}, ...), condition=%wide.region_7.8_spmd.clone, body=%wide.region_2.7_spmd.clone.sunk | while | flops 273682432 | bytes 8483165 | solution.py:106
  68.9 3.7 %conditional.3 = ((f32[512,1,2]{0,2,1:T(2,128)S(1)}, f32[512,1,2]{0,2,1:T(2,128)S(1)}, f32[512,1,2,128]{0,3,2,1:T(8,128)S(1)})) conditional(s32[]{:T(128)} %convert_element_type.207, (f32[512,1,2]{0,2,1:T(2,128)S(1)}, f32[512,1,2]{0,2,1:T(2,128)S(1)}, f32[512,1,2,128]{0,3,2,1:T(8,128)S(1)}) %tuple.68, (s32[]{:T(128)}, s32[]{:T(128)}, ...), branch_computations={%region_3.0_spmd, %region_4.6_spmd} | conditional | flops 273682432 | bytes 8480870 | solution.py:104
  69.0 0.2 broadcast_compare_fusion
  69.2 1.6 fusion.102
  70.8 1.5 fusion.5
  72.3 0.3 fusion.4
  73.0 0.1 divide_convert_fusion
  73.1 2.1 %convolution_convert_fusion.2 = bf16[512,2048]{1,0:T(8,128)(2,1)} fusion(bf16[512,256]{0,1:T(8,128)(2,1)S(1)} %bitcast.135, bf16[256,2048]{1,0:T(8,128)(2,1)S(1)} %copy-done), kind=kOutput, calls=%fused_computation.43 | convolution fusion | flops 537919488 | bytes 3407872 | tf_op jit(solution)/shard_map/dot_general | solution.py:112
  75.2 0.0 reduce-scatter.2.cloned.1.call-update
  75.2 1.1 slice_convert_fusion
  76.3 1.6 %slice_reduce_fusion.1 = (f32[4,192]{1,0:T(4,128)S(1)}, f32[4,192]{1,0:T(4,128)S(1)}, f32[4,192]{1,0:T(4,128)S(1)}, f32[4,192]{1,0:T(4,128)S(1)}, f32[4,192]{1,0:T(4,128)S(1)}, /*index=5*/f32[4,192]{1,0:T(4,128)S(1)}) fusion(f32[4,192,8]{2,1,0:T(8,128)S(1)} %slice_convert_fusion), kind=kLoop, calls=%fused_computation.88 | loop fusion | flops 7680 | bytes 43008 | tf_op jit(solution)/shard_map/slice | solution.py:444
  78.0 1.9 %convolution_convert_fusion = bf16[4,384,2048]{2,1,0:T(8,128)(2,1)S(1)} fusion(bf16[4,192,2176]{2,1,0:T(8,128)(2,1)S(1)} %bitcast.125, f32[4,192]{1,0:T(4,128)S(1)} %get-tuple-element.319, f32[4,192]{1,0:T(4,128)S(1)} %get-tuple-element.322), kind=kOutput, calls=%fused_computation.35 | convolution fusion | flops 1211990016 | bytes 9445376 | tf_op jit(solution)/shard_map/nrq,nrd->nqd/dot_general | solution.py:425
  79.9 0.7 slice.91.after_ref
  80.6 2.0 %copy-done.5 = bf16[4,384,2048]{2,1,0:T(8,128)(2,1)} copy-done((bf16[4,384,2048]{2,1,0:T(8,128)(2,1)}, bf16[4,384,2048]{2,1,0:T(8,128)(2,1)S(1)}, u32[]{:S(2)}) %copy-start.5) | copy-done | bytes 6291480
  82.6 5.3 %fusion.16 = f32[8,4,48,256]{3,2,1,0:T(8,128)S(1)} fusion(bf16[8,2048,256]{2,1,0:T(8,128)(2,1)} %param.29, bf16[4,8,48,2048]{3,2,1,0:T(8,128)(2,1)S(1)} %bitcast.130), kind=kOutput, calls=%fused_computation.27 | convolution fusion | flops 1610612736 | bytes 16252928 | tf_op jit(solution)/shard_map/nxcd,xdf->nxcf/dot_general | solution.py:432
  87.9 13.9 %convert_bitcast_fusion = bf16[4,8,48,2048]{3,2,0,1:T(8,128)(2,1)} fusion(bf16[8,256,2048]{2,1,0:T(8,128)(2,1)} %param.31, f32[8,4,48,256]{3,2,1,0:T(8,128)S(1)} %fusion.16, bf16[8,2048,256]{2,1,0:T(8,128)(2,1)} %param.30, bf16[4,8,48,2048]{3,2,1,0:T(8,128)(2,1)} %bitcast.131), kind=kOutput, calls=%fused_computation.30 | convolution fusion | flops 3226730496 | bytes 30932992 | tf_op jit(solution)/shard_map/nxcf,xfd->nxcd/dot_general | solution.py:437
  101.8 3.4 %copy.25 = bf16[4,8,48,2048]{3,2,1,0:T(8,128)(2,1)S(1)} copy(bf16[4,8,48,2048]{3,2,0,1:T(8,128)(2,1)} %convert_bitcast_fusion) | data formatting | bytes 12582912 | tf_op jit(solution)/shard_map/convert_element_type | solution.py:439
  105.1 1.9 %fusion.52 = f32[4,192,2048]{2,1,0:T(8,128)S(1)} fusion(bf16[4,384,2048]{2,1,0:T(8,128)(2,1)S(1)} %bitcast.128, f32[4,192]{1,0:T(4,128)S(1)} %get-tuple-element.318, f32[4,192]{1,0:T(4,128)S(1)} %get-tuple-element.319, f32[4,192]{1,0:T(4,128)S(1)} %get-tuple-element.321, f32[4,192]{1,0:T(4,128)S(1)} %get-tuple-element.322), kind=kOutput, calls=%fused_computation.70 | convolution fusion | flops 1209729024 | bytes 12595200 | tf_op jit(solution)/shard_map/nrq,nqd->nrd/dot_general | solution.py:447
  107.1 2.2 %add_convert_fusion.rows_ref = bf16[4,192,2048]{2,1,0:T(8,128)(2,1)S(1)} fusion(f32[4,192,2048]{2,1,0:T(8,128)S(1)} %fusion.52, bf16[4,384,2048]{2,1,0:T(8,128)(2,1)S(1)} %bitcast.129, f32[4,192]{1,0:T(4,128)S(1)} %get-tuple-element.320, f32[4,192]{1,0:T(4,128)S(1)} %get-tuple-element.317, f32[4,192]{1,0:T(4,128)S(1)} %get-tuple-element.319, ...), kind=kOutput, calls=%fused_computation.29 | convolution fusion | flops 1212874752 | bytes 15740928 | tf_op jit(solution)/shard_map/nrq,nqd->nrd/dot_general | solution.py:447
  109.3 44.2 %shard_map.150 = bf16[4,192,512]{2,1,0:T(8,128)(2,1)S(1)} custom-call(bf16[4,192,2048]{2,1,0:T(8,128)(2,1)S(1)} %add_convert_fusion.rows_ref, bf16[16,128]{1,0:T(8,128)(2,1)S(1)} %slice.91.after_ref), custom_call_target="tpu_custom_call" | custom-call | bytes 50000000 | tf_op jit(solution)/shard_map/pallas_call | solution.py:363
  153.6 1.4 fusion.45
  (48 shorter events, 0.3 us)
Async XLA Ops:
  7.2 65.9 %copy-start = (bf16[256,2048]{1,0:T(8,128)(2,1)S(1)}, bf16[256,2048]{1,0:T(8,128)(2,1)}, u32[]{:S(2)}) copy-start(bf16[256,2048]{1,0:T(8,128)(2,1)} %param.24) | copy-start | bytes 3145732
  7.2 9.4 %copy-start.8 = (f32[2,512]{1,0:T(2,128)S(1)}, f32[2,512]{1,0:T(2,128)}, u32[]{:S(2)}) copy-start(f32[2,512]{1,0:T(2,128)} %param.28) | copy-start | bytes 12292
  7.2 61.6 %all-gather.2.cloned.1.call-start = ((), (), s32[]{:S(2)}) async-start(), calls=%async_computation.1 | async-start | bytes 1310720 | tf_op jit(solution)/shard_map/all_gather | solution.py:90
  11.1 143.9 %reduce-scatter.2.cloned.1.call-start = ((), (), s32[]{:S(2)}) async-start(), calls=%async_computation.2 | async-start | bytes 2621440 | tf_op jit(solution)/shard_map/reduce_scatter | solution.py:495
  13.7 7.5 %copy-start.7 = (s32[2,512]{1,0:T(2,128)S(1)}, s32[2,512]{1,0:T(2,128)}, u32[]{:S(2)}) copy-start(s32[2,512]{1,0:T(2,128)} %param.27) | copy-start | bytes 12292
  13.7 8.2 %copy-start.4 = (bf16[512,2048]{1,0:T(8,128)(2,1)S(1)}, bf16[512,2048]{1,0:T(8,128)(2,1)}, u32[]{:S(2)}) copy-start(bf16[512,2048]{1,0:T(8,128)(2,1)} %param.25) | copy-start | bytes 6291460
  21.9 1.3 copy-start.9
  23.9 44.9 %copy-start.6 = (f32[2,2048]{1,0:T(2,128)S(1)}, f32[2,2048]{1,0:T(2,128)}, u32[]{:S(2)}) copy-start(f32[2,2048]{1,0:T(2,128)} %param.23) | copy-start | bytes 49156
  67.1 1.7 %copy-start.2 = (bf16[4,4,48,2176]{3,2,1,0:T(8,128)(2,1)}, bf16[4,4,48,2176]{3,2,1,0:T(8,128)(2,1)S(1)}, u32[]{:S(2)}) copy-start(bf16[4,4,48,2176]{3,2,1,0:T(8,128)(2,1)S(1)} %shard_map.149) | copy-start | bytes 10027012
  75.2 2.8 %copy-start.3 = (bf16[4,4,48,2176]{3,2,1,0:T(8,128)(2,1)S(1)}, bf16[4,4,48,2176]{3,2,1,0:T(8,128)(2,1)}, u32[]{:S(2)}) copy-start(bf16[4,4,48,2176]{3,2,1,0:T(8,128)(2,1)} %copy-done.2) | copy-start | bytes 10027012
  79.9 2.7 %copy-start.5 = (bf16[4,384,2048]{2,1,0:T(8,128)(2,1)}, bf16[4,384,2048]{2,1,0:T(8,128)(2,1)S(1)}, u32[]{:S(2)}) copy-start(bf16[4,384,2048]{2,1,0:T(8,128)(2,1)S(1)} %convolution_convert_fusion) | copy-start | bytes 18874372
  109.3 45.7 %copy-start.1 = (bf16[256,2048]{1,0:T(8,128)(2,1)S(1)}, bf16[256,2048]{1,0:T(8,128)(2,1)}, u32[]{:S(2)}) copy-start(bf16[256,2048]{1,0:T(8,128)(2,1)} %param.24) | copy-start | bytes 3145732
Sparse Core Ops, SparseCore 0:
  11.2 45.9 all-gather.1
  75.3 45.8 reduce-scatter.1
